TPU v7x, 32 devices: a whole 2x2x4 slice. The times are simulated.
32 devices in a mesh: sp: 8 (over z, x), tp: 4 (over y, core).
Axes of the slice: x: 2, y: 2, z: 4, core: 2. Of those that a mesh axis runs over, the one named last changes fastest.
Arguments:
- mixed: bfloat16 [1024, 2048], P('sp'), may hold values from -6 to 6
- cotangent: bfloat16 [1024, 2048], P('sp'), may hold values from -6 to 6
- routes: int32 [1024, 2], P('sp'), may hold values from 0 to 7, all different within a row; in each aligned block of 128 rows (0 to 127, 128 to 255, ...) at most 64 rows name the same one
- gates: float32 [1024, 2], P('sp'), may hold values from 0.1 to 1
- w_gate: bfloat16 [8, 2048, 1024], P('sp', None, 'tp'), may hold values from -0.125 to 0.125
- w_up: bfloat16 [8, 2048, 1024], P('sp', None, 'tp'), may hold values from -0.125 to 0.125
- w_down: bfloat16 [8, 1024, 2048], P('sp', 'tp'), may hold values from -0.1875 to 0.1875
- out_weight: bfloat16 [1024, 2048], P('tp'), may hold values from -0.1875 to 0.1875
- gate_pre: bfloat16 [1024, 1024], P('sp', 'tp'), may hold values from -8 to 8
- mixer_out: bfloat16 [1024, 1024], P('sp', 'tp'), may hold values from -6 to 6
- values: bfloat16 [1024, 1024], P('sp', 'tp'), may hold values from -6 to 6
- write_keys: bfloat16 [1024, 512], P('sp', 'tp'), may hold values from -1.25 to 1.25
- read_keys: bfloat16 [1024, 512], P('sp', 'tp'), may hold values from -1.25 to 1.25
- log_decay: float32 [16, 1024], P('tp', 'sp'), may hold values from -0.08 to 0
- entry_states: float32 [8, 16, 64, 128], P('sp', 'tp'), may hold values from -6 to 6
Outputs:
- d_w_gate: bfloat16 [8, 2048, 1024], P('sp', None, 'tp')
- d_w_up: bfloat16 [8, 2048, 1024], P('sp', None, 'tp')
- d_w_down: bfloat16 [8, 1024, 2048], P('sp', 'tp')
- d_out_weight: float32 [2048, 1024], P('sp', 'tp')
- d_input: bfloat16 [1024, 2048], P('sp', 'tp')
- d_values: bfloat16 [1024, 1024], P('sp', 'tp')
- d_write: float32 [1024, 512], P('sp', 'tp')
- d_read: float32 [1024, 512], P('sp', 'tp')
- d_gate: bfloat16 [1024, 1024], P('sp', 'tp')
Inputs may be any that keep to these rules, and one draw needn't show every extreme that they name: `routes`: each row names 2 different experts; in the 128 rows of one device no expert is named more than 64 times, and in some blocks one is named exactly 64 times.
All inputs are finite; a program needn't handle non-finite values.
Results may differ from a plain program's by a relative error of at most 0.0062.
Values may be sent and summed in bfloat16 or wider, within the bound.
A program may use at most 64 MiB of HBM per device.

v0:
```python
import jax
import jax.numpy as jnp
from jax import lax
from jax.sharding import PartitionSpec as P

D = 2048
HEAD_DIM = 64
BLOCK = 128
TOPK = 2
TOK_DEV = 128


precise = lax.Precision.HIGHEST


def prefix(part, axis, combine, identity):
    count = lax.axis_size(axis)
    place = lax.axis_index(axis)
    ahead = count - 1 - place
    gathered = jax.tree.map(lambda a: lax.all_gather(a, axis), part)
    state = jax.tree.map(lambda a, e: jnp.zeros_like(a) + jnp.asarray(e, a.dtype), part, identity)

    def one(lap, state):
        source = count - 1 - lap
        return combine(
            state, jax.tree.map(lambda a: lax.dynamic_index_in_dim(a, source, 0, False), gathered)
        )

    return lax.fori_loop(0, ahead, one, state)


def silu_grad(pre_act):
    logistic = jax.nn.sigmoid(pre_act)
    return logistic * (1.0 + pre_act * (1.0 - logistic))


def contract_rows(first_op, second_op):
    return lax.dot_general(
        first_op, second_op, (((0,), (0,)), ((), ())), preferred_element_type=jnp.float32
    )


def contract_cols(first_op, second_op):
    return lax.dot_general(
        first_op, second_op, (((1,), (1,)), ((), ())), preferred_element_type=jnp.float32
    )


def combine_state(earlier, later):
    return (later[0] * earlier[0], later[1] + later[0][:, None, None] * earlier[1])


def block_back(grad_state, inputs_x, grad_y, log_rate, write_rows, read_rows, start_state):
    block_len = log_rate.shape[0]
    running = jnp.cumsum(log_rate, axis=0)
    causal_mask = (jnp.arange(block_len)[:, None] >= jnp.arange(block_len)[None, :])[:, :, None]
    spread = running[:, None, :] - running[None, :, :]
    decay_mat = jnp.where(causal_mask, jnp.exp(jnp.where(causal_mask, spread, 0.0)), 0.0)
    intersection = jnp.dot(read_rows, write_rows.T, precision=precise)
    mixing = intersection[:, :, None] * decay_mat
    to_end = jnp.exp(running[-1][None, :] - running)
    from_start = jnp.exp(running)
    grad_x = jnp.einsum("lsj,ljp->sjp", mixing, grad_y, precision=precise) + to_end[
        :, :, None
    ] * jnp.einsum("sn,jpn->sjp", write_rows, grad_state, precision=precise)
    weighted = jnp.einsum("ljp,sjp->lsj", grad_y, inputs_x, precision=precise) * decay_mat
    grad_w = jnp.einsum("lsj,ln->sn", weighted, read_rows, precision=precise) + jnp.einsum(
        "sj,sjp,jpn->sn", to_end, inputs_x, grad_state, precision=precise
    )
    grad_r = jnp.einsum("lsj,sn->ln", weighted, write_rows, precision=precise) + jnp.einsum(
        "lj,ljp,jpn->ln", from_start, grad_y, start_state, precision=precise
    )
    earlier = jnp.exp(running[-1])[:, None, None] * grad_state + jnp.einsum(
        "lj,ljp,ln->jpn", from_start, grad_y, read_rows, precision=precise
    )
    return (earlier, grad_x, grad_w, grad_r)


def body(
    mixed,
    cotangent,
    routes,
    gates,
    w_gate,
    w_up,
    w_down,
    out_weight,
    gate_pre,
    mixer_out,
    values,
    write_keys,
    read_keys,
    log_decay,
    entry_states,
):
    sp_count = lax.axis_size("sp")
    tp_count = lax.axis_size("tp")
    capacity = 4 * TOK_DEV // sp_count
    assigned = TOK_DEV * TOPK
    picks = routes.reshape(assigned)
    onehot = (picks[:, None] == jnp.arange(sp_count, dtype=jnp.int32)[None, :]).astype(jnp.int32)
    earlier_same = jnp.cumsum(onehot, axis=0) - onehot
    slot_of = jnp.sum(earlier_same * onehot, axis=1)
    target = picks * capacity + slot_of
    anchor = (
        jnp.full((sp_count * capacity,), assigned, jnp.int32)
        .at[target]
        .set(jnp.arange(assigned, dtype=jnp.int32))
    )
    weight_g = w_gate[0]
    weight_u = w_up[0]
    weight_d = w_down[0]
    column_count = D // tp_count
    offset = lax.axis_index("tp") * column_count
    tok_slice = lax.dynamic_slice_in_dim(mixed, offset, column_count, 1)
    cot_slice = lax.dynamic_slice_in_dim(cotangent, offset, column_count, 1)
    columns = tok_slice.shape[1]
    scaled = (
        (gates[:, :, None] * cot_slice[:, None, :].astype(jnp.float32))
        .astype(jnp.bfloat16)
        .reshape(assigned, columns)
    )
    empty_row = jnp.zeros((1, columns), jnp.bfloat16)
    cot_buffer = jnp.concatenate([scaled, empty_row])[anchor].reshape(sp_count, capacity, columns)
    tok_buffer = jnp.concatenate([tok_slice, empty_row])[anchor // TOPK].reshape(
        sp_count, capacity, columns
    )
    tok_buffer, cot_buffer = (tok_buffer, cot_buffer)
    tok_part, cot_part = (
        lax.all_to_all(tok_buffer, "sp", split_axis=0, concat_axis=0, tiled=True),
        lax.all_to_all(cot_buffer, "sp", split_axis=0, concat_axis=0, tiled=True),
    )
    tok_rows, cot_rows = (
        lax.all_gather(tok_part, "tp", axis=2, tiled=True),
        lax.all_gather(cot_part, "tp", axis=2, tiled=True),
    )
    expert_tok_rows = tok_rows
    expert_cot_rows = cot_rows
    expert_tok_rows = expert_tok_rows.reshape(-1, D)
    expert_cot_rows = expert_cot_rows.reshape(-1, D)
    pre_gate = jnp.dot(expert_tok_rows, weight_g, preferred_element_type=jnp.float32)
    pre_up = jnp.dot(expert_tok_rows, weight_u, preferred_element_type=jnp.float32)
    active = jax.nn.silu(pre_gate)
    hidden = (active * pre_up).astype(jnp.bfloat16)
    grad_down = contract_rows(hidden, expert_cot_rows)
    grad_hidden = contract_cols(expert_cot_rows, weight_d)
    grad_gate = (grad_hidden * pre_up * silu_grad(pre_gate)).astype(jnp.bfloat16)
    grad_upval = (grad_hidden * active).astype(jnp.bfloat16)
    grad_wg = contract_rows(expert_tok_rows, grad_gate)
    grad_wu = contract_rows(expert_tok_rows, grad_upval)
    partial_value = contract_cols(grad_gate, weight_g) + contract_cols(grad_upval, weight_u)
    grad_wg, grad_wu, grad_down, partial_value = (grad_wg, grad_wu, grad_down, partial_value)
    row_total = partial_value.shape[0]
    pieces = partial_value.astype(jnp.bfloat16).reshape(row_total, tp_count, column_count)
    received = lax.all_to_all(pieces, "tp", split_axis=1, concat_axis=1, tiled=True)
    summed = (
        jnp.sum(received.astype(jnp.float32), axis=1)
        .astype(jnp.bfloat16)
        .reshape(sp_count, capacity, column_count)
    )
    returned = lax.all_to_all(summed, "sp", split_axis=0, concat_axis=0, tiled=True)
    columns = returned.shape[-1]
    picked = returned.reshape(sp_count * capacity, columns)[target].reshape(TOK_DEV, TOPK, columns)
    d_input = (cot_slice.astype(jnp.float32) + jnp.sum(picked.astype(jnp.float32), axis=1)).astype(
        jnp.bfloat16
    )
    whole = lax.all_gather(d_input, "tp", axis=1, tiled=True)
    back_proj = contract_cols(whole, out_weight)
    pre_act = gate_pre.astype(jnp.float32)
    gate_act = jax.nn.silu(pre_act)
    saved_out = mixer_out.astype(jnp.float32)
    d_gate = (back_proj * saved_out * silu_grad(pre_act)).astype(jnp.bfloat16)
    gated = (saved_out * gate_act).astype(jnp.bfloat16)
    d_out_weight = lax.psum_scatter(
        contract_rows(whole, gated), "sp", scatter_dimension=0, tiled=True
    )
    head_count = out_weight.shape[0] // HEAD_DIM
    grad_y = (back_proj * gate_act).reshape(TOK_DEV, head_count, HEAD_DIM)
    inputs_x = values.astype(jnp.float32).reshape(TOK_DEV, head_count, HEAD_DIM)
    write_rows = write_keys.astype(jnp.float32)
    read_rows = read_keys.astype(jnp.float32)
    log_rate = log_decay.T
    total_run = jnp.cumsum(log_rate, axis=0)
    shard_decay = jnp.exp(total_run[-1])
    shard_grad = jnp.einsum(
        "lj,ljp,ln->jpn", jnp.exp(total_run), grad_y, read_rows, precision=precise
    )
    identity = (jnp.ones_like(shard_decay), jnp.zeros_like(shard_grad))
    incoming = prefix((shard_decay, shard_grad), "sp", combine_state, identity)
    grad_state = incoming[1]
    pieces_x = []
    pieces_w = []
    pieces_r = []
    for block_id in reversed(range(TOK_DEV // BLOCK)):
        grad_state, grad_x, grad_w, grad_r = block_back(
            grad_state, inputs_x, grad_y, log_rate, write_rows, read_rows, entry_states[block_id]
        )
        pieces_x.insert(0, grad_x)
        pieces_w.insert(0, grad_w)
        pieces_r.insert(0, grad_r)
    d_values = pieces_x[0].reshape(TOK_DEV, head_count * HEAD_DIM).astype(jnp.bfloat16)
    d_write = pieces_w[0]
    d_read = pieces_r[0]
    return (
        grad_wg.astype(jnp.bfloat16)[None],
        grad_wu.astype(jnp.bfloat16)[None],
        grad_down.astype(jnp.bfloat16)[None],
        d_out_weight,
        d_input,
        d_values,
        d_write,
        d_read,
        d_gate,
    )


def solution(mesh):
    return jax.shard_map(
        body,
        mesh=mesh,
        in_specs=(
            P("sp", None),
            P("sp", None),
            P("sp", None),
            P("sp", None),
            P("sp", None, "tp"),
            P("sp", None, "tp"),
            P("sp", "tp", None),
            P("tp", None),
            P("sp", "tp"),
            P("sp", "tp"),
            P("sp", "tp"),
            P("sp", "tp"),
            P("sp", "tp"),
            P("tp", "sp"),
            P("sp", "tp", None, None),
        ),
        out_specs=(
            P("sp", None, "tp"),
            P("sp", None, "tp"),
            P("sp", "tp", None),
            P("sp", "tp"),
            P("sp", "tp"),
            P("sp", "tp"),
            P("sp", "tp"),
            P("sp", "tp"),
            P("sp", "tp"),
        ),
        check_vma=False,
    )
```

profile of v0, /device:TPU:0, one launch (start us, length us, event | category | flops | bytes accessed | tf_op | source)
XLA Modules:
  0.0 265.6 jit_solution(14270438159502153664)
XLA Ops:
  10.3 1.4 scatter_custom_fusion
  12.8 2.0 gather_fusion
  14.8 21.7 %all_to_all.20 = bf16[8,64,512]{2,1,0:T(8,128)(2,1)} all-to-all(bf16[8,64,512]{2,1,0:T(8,128)(2,1)S(1)} %bitcast.115), channel_id=1, replica_groups=mesh['sp'=8,'tp'=4] {'sp'}, dimensions={0} | all-to-all | bytes 1048576 | tf_op jit(solution)/shard_map/all_to_all | solution.py:130
  37.5 2.0 gather_fusion.1
  39.5 17.6 %all_to_all.21 = bf16[8,64,512]{2,1,0:T(8,128)(2,1)} all-to-all(bf16[8,64,512]{2,1,0:T(8,128)(2,1)S(1)} %bitcast.116), channel_id=1, replica_groups=mesh['sp'=8,'tp'=4] {'sp'}, dimensions={0} | all-to-all | bytes 1048576 | tf_op jit(solution)/shard_map/all_to_all | solution.py:131
  57.1 1.1 all-gather.6.cloned.1.call-done
  58.3 2.5 fusion.10
  61.5 20.9 %all-gather.8.cloned.1.call-done = bf16[8,64,2048]{2,1,0:T(8,128)(2,1)} async-done(((bf16[8,64,512]{2,1,0:T(8,128)(2,1)}), bf16[8,64,2048]{2,1,0:T(8,128)(2,1)}) %all-gather.8.cloned.1.call-update) | async-done | bytes 2097168 | tf_op jit(solution)/shard_map/all_gather | solution.py:135
  82.4 2.7 %multiply_convert_fusion.1 = (bf16[512,256]{1,0:T(8,128)(2,1)S(1)}, bf16[512,256]{1,0:T(8,128)(2,1)S(1)}) fusion(f32[512,256]{1,0:T(8,128)S(1)} %fusion.10, f32[512,256]{1,0:T(8,128)S(1)} %fusion.13, bf16[512,2048]{1,0:T(8,128)(2,1)} %bitcast.117, bf16[1,256,2048]{2,1,0:T(8,128)(2,1)} %param.23), kind=kOutput, calls=%fused_computation.36 | convolution fusion | flops 538574848 | bytes 4718592 | tf_op jit(solution)/shard_map/dot_general | solution.py:44
  86.8 28.1 %all_to_all.22 = bf16[512,4,512]{2,0,1:T(8,128)(2,1)S(1)} all-to-all(bf16[512,4,512]{2,0,1:T(8,128)(2,1)S(1)} %bitcast.113), channel_id=1, replica_groups=mesh['sp'=8,'tp'=4] {'tp'}, dimensions={1} | all-to-all | bytes 4194304 | tf_op jit(solution)/shard_map/all_to_all | solution.py:155
  114.9 1.2 reduce_sum.47
  116.2 5.5 %all-to-all-start.3 = ((bf16[8,64,512]{2,1,0:T(8,128)(2,1)}), bf16[8,64,512]{2,1,0:T(8,128)(2,1)S(1)}, u32[]{:S(2)}, u32[]{:S(2)}) async-start(bf16[8,64,512]{2,1,0:T(8,128)(2,1)} %bitcast.119), calls=%async_computation.3 | async-start | bytes 1048576 | tf_op jit(solution)/shard_map/all_to_all | solution.py:161
  122.1 13.7 %all-to-all-done.3 = bf16[8,64,512]{2,1,0:T(8,128)(2,1)S(1)} async-done(((bf16[8,64,512]{2,1,0:T(8,128)(2,1)}), bf16[8,64,512]{2,1,0:T(8,128)(2,1)S(1)}, u32[]{:S(2)}, u32[]{:S(2)}) %all-to-all-start.3) | async-done | bytes 524320 | tf_op jit(solution)/shard_map/all_to_all | solution.py:161
  135.8 1.2 gather_fusion.2
  138.9 6.5 %all_gather.21 = bf16[128,2048]{1,0:T(8,128)(2,1)S(1)} all-gather(bf16[128,512]{1,0:T(8,128)(2,1)S(1)} %add_convert_fusion.1), channel_id=1, replica_groups=mesh['sp'=8,'tp'=4] {'tp'}, dimensions={1}, use_global_device_ids=true | all-gather | bytes 655360 | tf_op jit(solution)/shard_map/all_gather | solution.py:167
  145.4 2.3 fusion.21
  149.0 1.8 fusion.39
  151.2 18.8 %all-gather.1 = f32[8,1,4]{2,1,0:T(1,128)S(1)} all-gather(f32[1,1,4]{2,1,0:T(1,128)S(1)} %get-tuple-element.153), channel_id=1, replica_groups=mesh['sp'=8,'tp'=4] {'sp'}, dimensions={0}, use_global_device_ids=true | all-gather | bytes 144 | tf_op jit(solution)/shard_map/all_gather | solution.py:20
  170.2 3.5 %fusion = bf16[1,2048,256]{2,1,0:T(8,128)(2,1)} fusion(bf16[512,2048]{1,0:T(8,128)(2,1)} %bitcast.134, bf16[512,256]{1,0:T(8,128)(2,1)S(1)} %get-tuple-element.147), kind=kOutput, calls=%fused_computation.10 | convolution fusion | flops 537395200 | bytes 3407872 | tf_op jit(solution)/shard_map/dot_general | solution.py:38
  173.7 1.7 fusion.1
  175.9 1.8 fusion.2
  179.3 8.7 %all-gather.10.cloned.1.call-done = f32[32,64,128]{2,1,0:T(8,128)} async-done(((f32[4,64,128]{2,1,0:T(8,128)}), f32[32,64,128]{2,1,0:T(8,128)}) %all-gather.10.cloned.1.call-update) | async-done | bytes 1048592 | tf_op jit(solution)/shard_map/all_gather | solution.py:20
  188.0 7.2 %while.14 = (s32[]{:T(128)}, f32[4,64,128]{2,1,0:T(8,128)S(1)}, s32[]{:T(128)}, f32[8,4,64,128]{3,2,1,0:T(8,128)}, f32[8,4]{1,0:T(8,128)S(1)}, /*index=5*/s32[]{:T(128)}, s32[]{:T(128)}, s32[]{:T(128)}, s32[]{:T(128)}) while((s32[]{:T(128)}, f32[4,64,128]{2,1,0:T(8,128)S(1)}, s32[]{:T(128)}, f32[8,4,64,128]{3,2,1,0:T(8,128)}, ...), condition=%wide.region_9.10_spmd, body=%wide.region_8.9_spmd.sunk | while | flops 65542 | bytes 393419 | solution.py:29
  198.0 61.1 %reduce-scatter.2.cloned.1.call-done = f32[256,256]{1,0:T(8,128)} async-done(((f32[2048,256]{1,0:T(8,128)}), f32[256,256]{1,0:T(8,128)}) %reduce-scatter.2.cloned.1.call-update) | async-done | bytes 262160 | tf_op jit(solution)/shard_map/reduce_scatter | solution.py:174
  (115 shorter events, 23.3 us)
Async XLA Ops:
  7.2 51.1 %copy-start = (bf16[1,2048,256]{2,1,0:T(8,128)(2,1)S(1)}, bf16[1,2048,256]{2,1,0:T(8,128)(2,1)}, u32[]{:S(2)}) copy-start(bf16[1,2048,256]{2,1,0:T(8,128)(2,1)} %param.21) | copy-start | bytes 3145732
  7.2 51.1 %all-gather.6.cloned.1.call-start = ((), (), s32[]{:S(2)}) async-start(), calls=%async_computation.5 | async-start | bytes 2621440 | tf_op jit(solution)/shard_map/all_gather | solution.py:134
  14.7 22.4 %copy-start.17 = (f32[128,2]{0,1:T(2,128)S(1)}, f32[128,2]{0,1:T(2,128)}, u32[]{:S(2)}) copy-start(f32[128,2]{0,1:T(2,128)} %param.20) | copy-start | bytes 3076
  36.5 45.9 %all-gather.8.cloned.1.call-start = ((), (), s32[]{:S(2)}) async-start(), calls=%async_computation.6 | async-start | bytes 2621440 | tf_op jit(solution)/shard_map/all_gather | solution.py:135
  57.1 3.6 %copy-start.2 = (bf16[1,2048,256]{2,1,0:T(8,128)(2,1)S(1)}, bf16[1,2048,256]{2,1,0:T(8,128)(2,1)}, u32[]{:S(2)}) copy-start(bf16[1,2048,256]{2,1,0:T(8,128)(2,1)} %param.22) | copy-start | bytes 3145732
  58.3 2.5 copy-start.18
  60.7 24.3 %copy-start.4 = (f32[512,256]{1,0:T(8,128)}, f32[512,256]{1,0:T(8,128)S(1)}, u32[]{:S(2)}) copy-start(f32[512,256]{1,0:T(8,128)S(1)} %fusion.10) | copy-start | bytes 1572868
  61.5 23.6 %copy-start.6 = (f32[512,256]{1,0:T(8,128)}, f32[512,256]{1,0:T(8,128)S(1)}, u32[]{:S(2)}) copy-start(f32[512,256]{1,0:T(8,128)S(1)} %fusion.13) | copy-start | bytes 1572868
  114.9 6.8 %copy-start.16 = (f32[4,128]{1,0:T(4,128)S(1)}, f32[4,128]{1,0:T(4,128)}, u32[]{:S(2)}) copy-start(f32[4,128]{1,0:T(4,128)} %param.30) | copy-start | bytes 6148
  116.2 19.7 %all-to-all-start.3 = ((bf16[8,64,512]{2,1,0:T(8,128)(2,1)}), bf16[8,64,512]{2,1,0:T(8,128)(2,1)S(1)}, u32[]{:S(2)}, u32[]{:S(2)}) async-start(bf16[8,64,512]{2,1,0:T(8,128)(2,1)} %bitcast.119), calls=%async_computation.3 | async-start | bytes 1048576 | tf_op jit(solution)/shard_map/all_to_all | solution.py:161
  121.7 66.3 %all-gather.10.cloned.1.call-start = ((), (), s32[]{:S(2)}) async-start(), calls=%async_computation.8 | async-start | bytes 1179648 | tf_op jit(solution)/shard_map/all_gather | solution.py:20
  135.8 9.6 %copy-start.13 = (bf16[128,256]{1,0:T(8,128)(2,1)S(1)}, bf16[128,256]{1,0:T(8,128)(2,1)}, u32[]{:S(2)}) copy-start(bf16[128,256]{1,0:T(8,128)(2,1)} %param.26) | copy-start | bytes 196612
  135.8 9.6 %copy-start.14 = (bf16[128,256]{1,0:T(8,128)(2,1)S(1)}, bf16[128,256]{1,0:T(8,128)(2,1)}, u32[]{:S(2)}) copy-start(bf16[128,256]{1,0:T(8,128)(2,1)} %param.25) | copy-start | bytes 196612
  137.3 10.5 %copy-start.9 = (bf16[128,128]{1,0:T(8,128)(2,1)S(1)}, bf16[128,128]{1,0:T(8,128)(2,1)}, u32[]{:S(2)}) copy-start(bf16[128,128]{1,0:T(8,128)(2,1)} %param.29) | copy-start | bytes 98308
  138.9 12.0 %copy-start.3 = (bf16[128,512]{1,0:T(8,128)(2,1)}, bf16[128,512]{1,0:T(8,128)(2,1)S(1)}, u32[]{:S(2)}) copy-start(bf16[128,512]{1,0:T(8,128)(2,1)S(1)} %add_convert_fusion.1) | copy-start | bytes 393220
  148.8 2.2 copy-start.15
  148.8 21.2 %copy-start.8 = (bf16[128,128]{1,0:T(8,128)(2,1)S(1)}, bf16[128,128]{1,0:T(8,128)(2,1)}, u32[]{:S(2)}) copy-start(bf16[128,128]{1,0:T(8,128)(2,1)} %param.28) | copy-start | bytes 98308
  148.8 110.2 %reduce-scatter.2.cloned.1.call-start = ((), (), s32[]{:S(2)}) async-start(), calls=%async_computation.7 | async-start | bytes 2359296 | tf_op jit(solution)/shard_map/reduce_scatter | solution.py:174
  170.2 3.5 %copy-start.11 = (bf16[512,256]{1,0:T(8,128)(2,1)S(1)}, bf16[512,256]{1,0:T(8,128)(2,1)}, u32[]{:S(2)}) copy-start(bf16[512,256]{1,0:T(8,128)(2,1)} %copy-done.10) | copy-start | bytes 786436
  170.2 3.5 %copy-start.19 = (bf16[8,64,2048]{2,1,0:T(8,128)(2,1)S(1)}, bf16[8,64,2048]{2,1,0:T(8,128)(2,1)}, u32[]{:S(2)}) copy-start(bf16[8,64,2048]{2,1,0:T(8,128)(2,1)} %all-gather.6.cloned.1.call-done) | copy-start | bytes 6291460
  173.7 1.8 copy-start.1
  173.7 1.8 copy-start.5
  173.7 2.2 copy-start.7
  175.9 1.8 copy-start.12
  (1 other events, 0.8 us)
Sparse Core Ops, SparseCore 0:
  36.6 21.5 all-gather.5
  59.8 22.5 all-gather.7
  148.9 38.9 all-gather.9
  191.9 67.0 reduce-scatter.1
where the time goes:
time: 266 us
  waiting for transfers between devices  106 us (40%)
  blocking collectives  92.8 us (35%)
  matrix products  23.1 us (9%)
  between operations  14.2 us (5%)
  other arithmetic  12.6 us (5%)
  local copies, waits for them, and re-layouts  11.2 us (4%)
  starting transfers between devices  5.85 us (2%)
    reduce_scatter x1, waiting for transfers between devices, body(): lax.psum_scatter(contract_rows(whole, gated), 'sp', scatter_dimension=0,...  61.1 us
    all_to_all x1, blocking collectives, body(): lax.all_to_all(pieces, 'tp', split_axis=1, concat_axis=1, tiled=True)  28.1 us
    all_to_all x1, blocking collectives, body(): lax.all_to_all(tok_buffer, 'sp', split_axis=0, concat_axis=0, tiled=True)  21.7 us
    all_gather x1, waiting for transfers between devices, body(): lax.all_gather(cot_part, 'tp', axis=2, tiled=True)  20.9 us
    all_gather x1, blocking collectives, prefix(): gathered = jax.tree.map(lambda a: lax.all_gather(a, axis), part)  18.8 us
    all_to_all x1, blocking collectives, body(): lax.all_to_all(cot_buffer, 'sp', split_axis=0, concat_axis=0, tiled=True)  17.6 us
    all_to_all x1, waiting for transfers between devices, body(): lax.all_to_all(summed, 'sp', split_axis=0, concat_axis=0, tiled=True)  13.7 us
    dot_general x4, matrix products, contract_rows(): lax.dot_general(first_op, second_op, (((0,), (0,)), ((), ())), preferred_...  8.79 us
  transfers between devices with their start and end apart: 5, of which 5 were waited for; matrix products, arithmetic and copies ran while one was open for 10% of the time, Pallas kernels for 0%

commit v1 on v0

--- a/solution.py
+++ b/solution.py
@@ -1,6 +1,10 @@
+import functools
+
 import jax
 import jax.numpy as jnp
 from jax import lax
+from jax.experimental import pallas as pl
+from jax.experimental.pallas import tpu as pltpu
 from jax.sharding import PartitionSpec as P
 
 D = 2048
@@ -13,20 +17,425 @@
 precise = lax.Precision.HIGHEST
 
 
-def prefix(part, axis, combine, identity):
-    count = lax.axis_size(axis)
-    place = lax.axis_index(axis)
-    ahead = count - 1 - place
-    gathered = jax.tree.map(lambda a: lax.all_gather(a, axis), part)
-    state = jax.tree.map(lambda a, e: jnp.zeros_like(a) + jnp.asarray(e, a.dtype), part, identity)
-
-    def one(lap, state):
-        source = count - 1 - lap
-        return combine(
-            state, jax.tree.map(lambda a: lax.dynamic_index_in_dim(a, source, 0, False), gathered)
+MESH_ID = pl.DeviceIdType.MESH
+VMEM = pl.BlockSpec(memory_space=pltpu.VMEM)
+
+
+def cols(t, width):
+    return pl.ds(pl.multiple_of(t * width, width), width)
+
+
+def signed_step(i):
+    return (i // 2 + 1) * (1 - 2 * (i % 2))
+
+
+def greet(n, m, me, t):
+    barrier = pltpu.get_barrier_semaphore()
+
+    @pl.loop(1, n)
+    def _(d):
+        pl.semaphore_signal(barrier, inc=1, device_id=((me + d) % n, t), device_id_type=MESH_ID)
+
+    @pl.loop(1, m // 2)
+    def _(d):
+        pl.semaphore_signal(barrier, inc=1, device_id=(me, (t + 2 * d) % m), device_id_type=MESH_ID)
+
+    pl.semaphore_signal(barrier, inc=1, device_id=(me, sibling(t)), device_id_type=MESH_ID)
+    pl.semaphore_wait(barrier, n - 1 + m // 2)
+
+
+def sibling(t):
+    return t + 1 - 2 * (t % 2)
+
+
+def remote(src, dst, send_sem, recv_sem, device):
+    return pltpu.make_async_remote_copy(
+        src_ref=src,
+        dst_ref=dst,
+        send_sem=send_sem,
+        recv_sem=recv_sem,
+        device_id=device,
+        device_id_type=MESH_ID,
+    )
+
+
+class Spread:
+    def __init__(self, n, m, me, t, buf, place, sems):
+        self.n, self.m, self.me, self.t = n, m, me, t
+        self.buf, self.place = buf, place
+        self.recv, self.first, self.share, self.relay, self.own = sems
+
+    @staticmethod
+    def scratch(n, m):
+        dma = pltpu.SemaphoreType.DMA
+        return [dma((n, m)), dma((n,)), dma((n, m // 2)), dma((n, m // 2)), dma((1,))]
+
+    def across(self, p):
+        me, t = self.me, self.t
+        return remote(
+            self.buf.at[p], self.place(me, t), self.first.at[p], self.recv.at[me, t], (p, t)
         )
 
-    return lax.fori_loop(0, ahead, one, state)
+    def arrived(self, j, t):
+        spot = self.place(j, t)
+        remote(spot, spot, self.first.at[0], self.recv.at[j, t], (self.me, self.t)).wait_recv()
+
+    def source(self, j, own):
+        return self.buf.at[j] if own else self.place(j, self.t)
+
+    def shared(self, j, d, own):
+        me, t, m = self.me, self.t, self.m
+        target = sibling(t) if d == 0 else (t + 2 * d) % m
+        return remote(
+            self.source(j, own),
+            self.place(j, t),
+            self.share.at[j, d],
+            self.recv.at[j, t],
+            (me, target),
+        )
+
+    def relayed(self, j, d):
+        me, t, m = self.me, self.t, self.m
+        origin = (t + 2 * d) % m
+        spot = self.place(j, origin)
+        return remote(spot, spot, self.relay.at[j, d], self.recv.at[j, origin], (me, sibling(t)))
+
+    def mine(self):
+        return pltpu.make_async_copy(
+            self.buf.at[self.me], self.place(self.me, self.t), self.own.at[0]
+        )
+
+    def begin(self):
+        @pl.loop(0, self.n - 1)
+        def _(i):
+            self.across((self.me + signed_step(i) + self.n) % self.n).start()
+
+    def begin_own(self):
+        for d in range(1, self.m // 2):
+            self.shared(self.me, d, True).start()
+        self.shared(self.me, 0, True).start()
+        self.mine().start()
+
+    def origin_of(self, i):
+        return (self.me - signed_step(i) + self.n) % self.n
+
+    def hand_on(self):
+        half = self.m // 2
+
+        def relay(j):
+            for d in range(1, half):
+                self.arrived(j, (self.t + 2 * d) % self.m)
+                self.relayed(j, d).start()
+
+        @pl.loop(0, self.n - 1)
+        def _(i):
+            j = self.origin_of(i)
+            self.arrived(j, self.t)
+            for d in range(1, half):
+                self.shared(j, d, False).start()
+            self.shared(j, 0, False).start()
+
+            @pl.when(i == 0)
+            def _():
+                relay(self.me)
+
+            @pl.when(i > 0)
+            def _():
+                relay(self.origin_of(i - 1))
+
+        relay(self.origin_of(self.n - 2))
+
+    def finish(self):
+        n, m, half = self.n, self.m, self.m // 2
+        self.mine().wait()
+        for d in range(half):
+            self.shared(self.me, d, True).wait_send()
+
+        @pl.loop(0, n - 1)
+        def _(i):
+            self.across((self.me + signed_step(i) + n) % n).wait_send()
+            j = self.origin_of(i)
+            for d in range(half):
+                self.shared(j, d, False).wait_send()
+
+        @pl.loop(0, n)
+        def _(j):
+            for d in range(1, half):
+                self.relayed(j, d).wait_send()
+            for d in range(half):
+                self.arrived(j, (sibling(self.t) + 2 * d) % m)
+
+
+def dispatch_kernel(n, m, tok_ref, cot_ref, tok_out, cot_out, *sems):
+    me, t = lax.axis_index("sp"), lax.axis_index("tp")
+    width = tok_ref.shape[2]
+    half = len(sems) // 2
+    tok = Spread(n, m, me, t, tok_ref, lambda j, q: tok_out.at[j, :, cols(q, width)], sems[:half])
+    cot = Spread(n, m, me, t, cot_ref, lambda j, q: cot_out.at[j, :, cols(q, width)], sems[half:])
+    greet(n, m, me, t)
+    tok.begin()
+    tok.begin_own()
+    cot.begin()
+    cot.begin_own()
+    tok.hand_on()
+    cot.hand_on()
+    tok.finish()
+    cot.finish()
+
+
+def dispatch(n, m, tok_buffer, cot_buffer):
+    cap, width = tok_buffer.shape[1:]
+    out = jax.ShapeDtypeStruct((n, cap, width * m), tok_buffer.dtype)
+    return pl.pallas_call(
+        functools.partial(dispatch_kernel, n, m),
+        out_shape=(out, out),
+        in_specs=[VMEM] * 2,
+        out_specs=(VMEM, VMEM),
+        scratch_shapes=Spread.scratch(n, m) * 2,
+        compiler_params=pltpu.CompilerParams(collective_id=0, has_side_effects=True),
+        name="dispatch",
+    )(tok_buffer, cot_buffer)
+
+
+def giveback_kernel(
+    n, m, part_ref, pick_ref, cot_ref, gated_ref,
+    whole_out, slice_out, gated_out,
+    sib, away, near, leave, back,
+    sib_send, sib_recv, away_send, near_recv, leave_send, back_recv,
+    gated_send, gated_recv, gated_own, share_send, share_recv, relay_send,
+):
+    me, t = lax.axis_index("sp"), lax.axis_index("tp")
+    half = m // 2
+    width = cot_ref.shape[1]
+    cap = part_ref.shape[1]
+    other = sibling(t)
+    f32 = jnp.float32
+    greet(n, m, me, t)
+
+    def to_sibling(d):
+        return remote(
+            part_ref.at[:, :, cols((other + 2 * d) % m, width)],
+            sib.at[d],
+            sib_send.at[d],
+            sib_recv.at[d],
+            (me, other),
+        )
+
+    def to_gated(p):
+        return remote(gated_ref, gated_out.at[me], gated_send.at[p], gated_recv.at[me], (p, t))
+
+    def to_column(j, d):
+        return remote(
+            away.at[d, j],
+            near.at[d, j],
+            away_send.at[d, j],
+            near_recv.at[d, j],
+            (me, (t + 2 * d) % m),
+        )
+
+    def to_home(j):
+        return remote(leave.at[j], back.at[me], leave_send.at[j], back_recv.at[me], (j, t))
+
+    order = lambda i: (me + signed_step(n - 2 - i) + n) % n
+
+    for d in list(range(1, half)) + [0]:
+        to_sibling(d).start()
+    keep = pltpu.make_async_copy(gated_ref, gated_out.at[me], gated_own.at[0])
+    keep.start()
+
+    @pl.loop(0, n - 1)
+    def _(i):
+        to_gated(order(i)).start()
+
+    for d in list(range(1, half)) + [0]:
+        to_sibling(d).wait_recv()
+
+    def pair_sum(j, d):
+        q = (t + 2 * d) % m
+        return part_ref[j, :, cols(q, width)].astype(f32) + sib[d, j].astype(f32)
+
+    def fill(j):
+        for d in range(1, half):
+            away[d, j] = pair_sum(j, d).astype(jnp.bfloat16)
+
+    def ship(j):
+        for d in range(1, half):
+            to_column(j, d).start()
+
+    fill(order(0))
+
+    @pl.loop(1, n - 1)
+    def _(i):
+        fill(order(i))
+        ship(order(i - 1))
+
+    fill(me)
+    ship(order(n - 2))
+
+    def total(j):
+        acc = pair_sum(j, 0)
+        for d in range(1, half):
+            spot = near.at[d, j]
+            remote(spot, spot, away_send.at[d, j], near_recv.at[d, j], (me, t)).wait_recv()
+            acc = acc + near[d, j].astype(f32)
+        return acc.astype(jnp.bfloat16)
+
+    leave[order(0)] = total(order(0))
+    ship(me)
+
+    @pl.loop(1, n - 1)
+    def _(i):
+        leave[order(i)] = total(order(i))
+        to_home(order(i - 1)).start()
+
+    back[me] = total(me)
+    to_home(order(n - 2)).start()
+
+    @pl.loop(0, n - 1)
+    def _(i):
+        j = order(i)
+        spot = back.at[j]
+        remote(spot, spot, leave_send.at[j], back_recv.at[j], (me, t)).wait_recv()
+
+    added = jnp.dot(pick_ref[...], back[...].reshape(n * cap, width), preferred_element_type=f32)
+    result = (cot_ref[...].astype(f32) + added).astype(jnp.bfloat16)
+    slice_out[...] = result
+    whole_out[:, cols(t, width)] = result
+
+    def spread(d):
+        return remote(
+            slice_out,
+            whole_out.at[:, cols(t, width)],
+            share_send.at[d],
+            share_recv.at[t],
+            (me, other if d == 0 else (t + 2 * d) % m),
+        )
+
+    def relay(d):
+        q = (t + 2 * d) % m
+        spot = whole_out.at[:, cols(q, width)]
+        return remote(spot, spot, relay_send.at[d], share_recv.at[q], (me, other))
+
+    def landed(q):
+        spot = whole_out.at[:, cols(q, width)]
+        remote(spot, spot, share_send.at[0], share_recv.at[q], (me, t)).wait_recv()
+
+    for d in list(range(1, half)) + [0]:
+        spread(d).start()
+    for d in range(1, half):
+        landed((t + 2 * d) % m)
+        relay(d).start()
+    for d in range(half):
+        landed((other + 2 * d) % m)
+    for d in range(half):
+        spread(d).wait_send()
+        to_sibling(d).wait_send()
+    for d in range(1, half):
+        relay(d).wait_send()
+
+    @pl.loop(0, n - 1)
+    def _(i):
+        j = order(i)
+        to_gated(j).wait_send()
+        to_home(j).wait_send()
+        spot = gated_out.at[j]
+        remote(spot, spot, gated_send.at[j], gated_recv.at[j], (me, t)).wait_recv()
+
+    @pl.loop(0, n)
+    def _(j):
+        for d in range(1, half):
+            to_column(j, d).wait_send()
+
+    keep.wait()
+
+
+def giveback(n, m, part, pick, cot_slice, gated):
+    cap = part.shape[1]
+    rows, width = cot_slice.shape
+    half = m // 2
+    bf16, dma = jnp.bfloat16, pltpu.SemaphoreType.DMA
+    return pl.pallas_call(
+        functools.partial(giveback_kernel, n, m),
+        out_shape=(
+            jax.ShapeDtypeStruct((rows, width * m), bf16),
+            jax.ShapeDtypeStruct((rows, width), bf16),
+            jax.ShapeDtypeStruct((n,) + gated.shape, bf16),
+        ),
+        in_specs=[VMEM] * 4,
+        out_specs=(VMEM,) * 3,
+        scratch_shapes=[
+            pltpu.VMEM((half, n, cap, width), bf16),
+            pltpu.VMEM((half, n, cap, width), bf16),
+            pltpu.VMEM((half, n, cap, width), bf16),
+            pltpu.VMEM((n, cap, width), bf16),
+            pltpu.VMEM((n, cap, width), bf16),
+            dma((half,)), dma((half,)), dma((half, n)), dma((half, n)), dma((n,)), dma((n,)),
+            dma((n,)), dma((n,)), dma((1,)), dma((half,)), dma((m,)), dma((half,)),
+        ],
+        compiler_params=pltpu.CompilerParams(collective_id=1, has_side_effects=True),
+        name="giveback",
+    )(part, pick, cot_slice, gated)
+
+
+def later_kernel(
+    n, m, grad_ref, decay_ref, rows_ref, state_out, rows_out,
+    held, rates, grad_send, grad_recv, rate_send, rate_recv, *sems,
+):
+    me, t = lax.axis_index("sp"), lax.axis_index("tp")
+    rows = Spread(n, m, me, t, rows_ref, lambda j, q: rows_out.at[j, q], sems)
+    greet(n, m, me, t)
+
+    def grad_to(p):
+        return remote(grad_ref, held.at[me], grad_send.at[p], grad_recv.at[me], (p, t))
+
+    def rate_to(p):
+        return remote(decay_ref, rates.at[me], rate_send.at[p], rate_recv.at[me], (p, t))
+
+    rows.begin()
+    rows.begin_own()
+
+    @pl.loop(0, me)
+    def _(p):
+        rate_to(p).start()
+        grad_to(p).start()
+
+    rows.hand_on()
+    state_out[...] = jnp.zeros_like(state_out)
+
+    @pl.loop(0, n - 1 - me)
+    def _(i):
+        j = n - 1 - i
+        spot, rate = held.at[j], rates.at[j]
+        remote(rate, rate, rate_send.at[j], rate_recv.at[j], (me, t)).wait_recv()
+        remote(spot, spot, grad_send.at[j], grad_recv.at[j], (me, t)).wait_recv()
+        state_out[...] = rates[j][:, None, :] * state_out[...] + held[j].astype(jnp.float32)
+
+    @pl.loop(0, me)
+    def _(p):
+        rate_to(p).wait_send()
+        grad_to(p).wait_send()
+
+    rows.finish()
+
+
+def later(n, m, grad, decay, rows):
+    dma = pltpu.SemaphoreType.DMA
+    return pl.pallas_call(
+        functools.partial(later_kernel, n, m),
+        out_shape=(
+            jax.ShapeDtypeStruct(grad.shape, jnp.float32),
+            jax.ShapeDtypeStruct((n, m) + rows.shape[1:], rows.dtype),
+        ),
+        in_specs=[VMEM] * 3,
+        out_specs=(VMEM,) * 2,
+        scratch_shapes=[
+            pltpu.VMEM((n,) + grad.shape, grad.dtype),
+            pltpu.VMEM((n,) + decay.shape, decay.dtype),
+            dma((n,)), dma((n,)), dma((n,)), dma((n,)),
+        ] + Spread.scratch(n, m),
+        compiler_params=pltpu.CompilerParams(collective_id=2, has_side_effects=True),
+        name="later",
+    )(grad, decay, rows)
 
 
 def silu_grad(pre_act):
@@ -44,10 +453,6 @@
     return lax.dot_general(
         first_op, second_op, (((1,), (1,)), ((), ())), preferred_element_type=jnp.float32
     )
-
-
-def combine_state(earlier, later):
-    return (later[0] * earlier[0], later[1] + later[0][:, None, None] * earlier[1])
 
 
 def block_back(grad_state, inputs_x, grad_y, log_rate, write_rows, read_rows, start_state):
@@ -101,12 +506,10 @@
     onehot = (picks[:, None] == jnp.arange(sp_count, dtype=jnp.int32)[None, :]).astype(jnp.int32)
     earlier_same = jnp.cumsum(onehot, axis=0) - onehot
     slot_of = jnp.sum(earlier_same * onehot, axis=1)
-    target = picks * capacity + slot_of
-    anchor = (
-        jnp.full((sp_count * capacity,), assigned, jnp.int32)
-        .at[target]
-        .set(jnp.arange(assigned, dtype=jnp.int32))
-    )
+    target = (picks * capacity + slot_of).reshape(TOK_DEV, TOPK)
+    slots = jnp.arange(sp_count * capacity, dtype=jnp.int32)[None, :]
+    chosen = [(target[:, k : k + 1] == slots).astype(jnp.bfloat16) for k in range(TOPK)]
+    pick = sum(chosen[1:], chosen[0])
     weight_g = w_gate[0]
     weight_u = w_up[0]
     weight_d = w_down[0]
@@ -114,28 +517,20 @@
     offset = lax.axis_index("tp") * column_count
     tok_slice = lax.dynamic_slice_in_dim(mixed, offset, column_count, 1)
     cot_slice = lax.dynamic_slice_in_dim(cotangent, offset, column_count, 1)
-    columns = tok_slice.shape[1]
-    scaled = (
-        (gates[:, :, None] * cot_slice[:, None, :].astype(jnp.float32))
-        .astype(jnp.bfloat16)
-        .reshape(assigned, columns)
-    )
-    empty_row = jnp.zeros((1, columns), jnp.bfloat16)
-    cot_buffer = jnp.concatenate([scaled, empty_row])[anchor].reshape(sp_count, capacity, columns)
-    tok_buffer = jnp.concatenate([tok_slice, empty_row])[anchor // TOPK].reshape(
-        sp_count, capacity, columns
-    )
-    tok_buffer, cot_buffer = (tok_buffer, cot_buffer)
-    tok_part, cot_part = (
-        lax.all_to_all(tok_buffer, "sp", split_axis=0, concat_axis=0, tiled=True),
-        lax.all_to_all(cot_buffer, "sp", split_axis=0, concat_axis=0, tiled=True),
-    )
-    tok_rows, cot_rows = (
-        lax.all_gather(tok_part, "tp", axis=2, tiled=True),
-        lax.all_gather(cot_part, "tp", axis=2, tiled=True),
-    )
-    expert_tok_rows = tok_rows
-    expert_cot_rows = cot_rows
+    scaled = [
+        (gates[:, k : k + 1] * cot_slice.astype(jnp.float32)).astype(jnp.bfloat16)
+        for k in range(TOPK)
+    ]
+    tok_buffer = contract_rows(pick, tok_slice).astype(jnp.bfloat16)
+    cot_buffer = contract_rows(
+        jnp.concatenate(chosen, axis=0), jnp.concatenate(scaled, axis=0)
+    ).astype(jnp.bfloat16)
+    expert_tok_rows, expert_cot_rows = dispatch(
+        sp_count,
+        tp_count,
+        tok_buffer.reshape(sp_count, capacity, column_count),
+        cot_buffer.reshape(sp_count, capacity, column_count),
+    )
     expert_tok_rows = expert_tok_rows.reshape(-1, D)
     expert_cot_rows = expert_cot_rows.reshape(-1, D)
     pre_gate = jnp.dot(expert_tok_rows, weight_g, preferred_element_type=jnp.float32)
@@ -149,31 +544,20 @@
     grad_wg = contract_rows(expert_tok_rows, grad_gate)
     grad_wu = contract_rows(expert_tok_rows, grad_upval)
     partial_value = contract_cols(grad_gate, weight_g) + contract_cols(grad_upval, weight_u)
-    grad_wg, grad_wu, grad_down, partial_value = (grad_wg, grad_wu, grad_down, partial_value)
-    row_total = partial_value.shape[0]
-    pieces = partial_value.astype(jnp.bfloat16).reshape(row_total, tp_count, column_count)
-    received = lax.all_to_all(pieces, "tp", split_axis=1, concat_axis=1, tiled=True)
-    summed = (
-        jnp.sum(received.astype(jnp.float32), axis=1)
-        .astype(jnp.bfloat16)
-        .reshape(sp_count, capacity, column_count)
-    )
-    returned = lax.all_to_all(summed, "sp", split_axis=0, concat_axis=0, tiled=True)
-    columns = returned.shape[-1]
-    picked = returned.reshape(sp_count * capacity, columns)[target].reshape(TOK_DEV, TOPK, columns)
-    d_input = (cot_slice.astype(jnp.float32) + jnp.sum(picked.astype(jnp.float32), axis=1)).astype(
-        jnp.bfloat16
-    )
-    whole = lax.all_gather(d_input, "tp", axis=1, tiled=True)
-    back_proj = contract_cols(whole, out_weight)
     pre_act = gate_pre.astype(jnp.float32)
     gate_act = jax.nn.silu(pre_act)
     saved_out = mixer_out.astype(jnp.float32)
+    gated = (saved_out * gate_act).astype(jnp.bfloat16)
+    whole, d_input, all_gated = giveback(
+        sp_count,
+        tp_count,
+        partial_value.astype(jnp.bfloat16).reshape(sp_count, capacity, D),
+        pick,
+        cot_slice,
+        gated,
+    )
+    back_proj = contract_cols(whole, out_weight)
     d_gate = (back_proj * saved_out * silu_grad(pre_act)).astype(jnp.bfloat16)
-    gated = (saved_out * gate_act).astype(jnp.bfloat16)
-    d_out_weight = lax.psum_scatter(
-        contract_rows(whole, gated), "sp", scatter_dimension=0, tiled=True
-    )
     head_count = out_weight.shape[0] // HEAD_DIM
     grad_y = (back_proj * gate_act).reshape(TOK_DEV, head_count, HEAD_DIM)
     inputs_x = values.astype(jnp.float32).reshape(TOK_DEV, head_count, HEAD_DIM)
@@ -185,9 +569,20 @@
     shard_grad = jnp.einsum(
         "lj,ljp,ln->jpn", jnp.exp(total_run), grad_y, read_rows, precision=precise
     )
-    identity = (jnp.ones_like(shard_decay), jnp.zeros_like(shard_grad))
-    incoming = prefix((shard_decay, shard_grad), "sp", combine_state, identity)
-    grad_state = incoming[1]
+    share = TOK_DEV // tp_count
+    own_rows = lax.dynamic_slice_in_dim(whole, lax.axis_index("tp") * share, share, 0)
+    own_rows = own_rows.reshape(share, sp_count, D // sp_count).transpose(1, 0, 2)
+    grad_state, all_rows = later(
+        sp_count,
+        tp_count,
+        shard_grad.astype(jnp.bfloat16),
+        jnp.broadcast_to(shard_decay[:, None], (head_count, shard_grad.shape[2])),
+        own_rows,
+    )
+    d_out_weight = contract_rows(
+        all_rows.reshape(sp_count * TOK_DEV, D // sp_count),
+        all_gated.reshape(sp_count * TOK_DEV, all_gated.shape[2]),
+    )
     pieces_x = []
     pieces_w = []
     pieces_r = []

time: 266 us -> 142 us (0.53)
  waiting for transfers between devices: 106 us -> 0 us
  Pallas kernels: 0 us -> 104 us
  blocking collectives: 92.8 us -> 0 us
  between operations: 14.2 us -> 0.96 us
  other arithmetic: 12.6 us -> 4.29 us
  starting transfers between devices: 5.85 us -> 0 us
  local copies, waits for them, and re-layouts: 11.2 us -> 7.7 us
    pallas_call x0 -> x3, Pallas kernels: none -> 104 us  [the longest x1 47.5 us: dispatch(): pl.pallas_call(functools.partial(dispatch_kernel, n, m), out_shape=(out,...]
    all_to_all x3 -> x0, blocking collectives: 67.5 us -> none  [the longest x1 28.1 us: body(): lax.all_to_all(pieces, 'tp', split_axis=1, concat_axis=1, tiled=True)]
    reduce_scatter x1 -> x0, waiting for transfers between devices: 61.1 us -> none  [body(): lax.psum_scatter(contract_rows(whole, gated), 'sp', scatter_dimension=0,...]
    all_gather x3 -> x0, waiting for transfers between devices: 30.7 us -> none  [the longest x1 20.9 us: body(): lax.all_gather(cot_part, 'tp', axis=2, tiled=True)]
    all_gather x2 -> x0, blocking collectives: 25.3 us -> none  [the longest x1 18.8 us: prefix(): gathered = jax.tree.map(lambda a: lax.all_gather(a, axis), part)]
    all_to_all x1 -> x0, waiting for transfers between devices: 13.7 us -> none  [body(): lax.all_to_all(summed, 'sp', split_axis=0, concat_axis=0, tiled=True)]
    all_to_all x1 -> x0, starting transfers between devices: 5.51 us -> none  [body(): lax.all_to_all(summed, 'sp', split_axis=0, concat_axis=0, tiled=True)]
    add x7 -> x2, other arithmetic: 6.97 us -> 1.48 us  [the longest x1 0.77 us: body(): pick = sum(chosen[1:], chosen[0])]
  transfers between devices with their start and end apart: 5 -> 0, of which waited for: 5 -> 0; matrix products, arithmetic and copies ran while one was open for 10% -> 0% of each run, Pallas kernels for 0% -> 0%
where the time goes in v1:
time: 142 us
  Pallas kernels  104 us (73%)
  matrix products  25.1 us (18%)
  local copies, waits for them, and re-layouts  7.7 us (5%)
  other arithmetic  4.29 us (3%)
    pallas_call x1, Pallas kernels, dispatch(): pl.pallas_call(functools.partial(dispatch_kernel, n, m), out_shape=(out,...  47.5 us
    pallas_call x1, Pallas kernels, giveback(): pl.pallas_call(functools.partial(giveback_kernel, n, m), out_shape=(jax.S...  35.4 us
    pallas_call x1, Pallas kernels, later(): pl.pallas_call(functools.partial(later_kernel, n, m), out_shape=(jax.Shap...  21.2 us
    dot_general x6, matrix products, contract_rows(): lax.dot_general(first_op, second_op, (((0,), (0,)), ((), ())), preferred_...  10.6 us
    dot_general x4, matrix products, contract_cols(): lax.dot_general(first_op, second_op, (((1,), (1,)), ((), ())), preferred_...  5.86 us
    unnamed x38, local copies, waits for them, and re-layouts  3.62 us

profile of v1, /device:TPU:0, one launch (start us, length us, event | category | flops | bytes accessed | tf_op | source)
XLA Modules:
  0.0 142.1 jit_solution(2781376628659323873)
XLA Ops:
  0.7 0.9 copy.60
  3.7 2.1 %convolution_convert_fusion.4 = bf16[512,512]{1,0:T(8,128)(2,1)} fusion(bf16[128,2048]{1,0:T(8,128)(2,1)} %param.15, s32[]{:T(128)S(6)} %select_n.14, s32[128]{0:T(128)S(1)} %get-tuple-element.70, s32[128]{0:T(128)S(1)} %get-tuple-element.69), kind=kOutput, calls=%fused_computation.8 | convolution fusion | flops 67895296 | bytes 656388 | tf_op jit(solution)/shard_map/dot_general | solution.py:447
  5.9 0.8 slice_bitcast_fusion.1
  6.7 1.0 fusion.18
  7.8 1.1 convolution_convert_fusion.3
  8.9 47.5 %dispatch.1 = (bf16[8,64,2048]{2,1,0:T(8,128)(2,1)}, bf16[8,64,2048]{2,1,0:T(8,128)(2,1)}) custom-call(bf16[8,64,512]{2,1,0:T(8,128)(2,1)} %bitcast.116, bf16[8,64,512]{2,1,0:T(8,128)(2,1)} %bitcast.122), custom_call_target="tpu_custom_call" | custom-call | tf_op jit(solution)/shard_map/dispatch/pallas_call | solution.py:189
  56.4 2.5 %fusion.10 = f32[512,256]{1,0:T(8,128)S(1)} fusion(bf16[512,2048]{1,0:T(8,128)(2,1)} %bitcast.130, bf16[1,2048,256]{2,1,0:T(8,128)(2,1)S(1)} %copy-done), kind=kOutput, calls=%fused_computation.24 | convolution fusion | flops 536870912 | bytes 3670016 | tf_op jit(solution)/shard_map/dot_general | solution.py:536
  59.6 0.9 copy-done.1
  60.8 0.8 multiply_convert_fusion.1
  61.6 1.7 %fusion = bf16[1,2048,256]{2,1,0:T(8,128)(2,1)} fusion(bf16[512,2048]{1,0:T(8,128)(2,1)S(1)} %bitcast.132, bf16[512,256]{1,0:T(8,128)(2,1)S(1)} %get-tuple-element.62), kind=kOutput, calls=%fused_computation.4 | convolution fusion | flops 537395200 | bytes 3407872 | tf_op jit(solution)/shard_map/dot_general | solution.py:447
  63.3 1.7 %fusion.1 = bf16[1,2048,256]{2,1,0:T(8,128)(2,1)} fusion(bf16[512,2048]{1,0:T(8,128)(2,1)S(1)} %bitcast.133, bf16[512,256]{1,0:T(8,128)(2,1)S(1)} %get-tuple-element.61), kind=kOutput, calls=%fused_computation.5 | convolution fusion | flops 537395200 | bytes 3407872 | tf_op jit(solution)/shard_map/dot_general | solution.py:447
  65.1 1.8 %fusion.2 = bf16[1,256,2048]{2,1,0:T(8,128)(2,1)} fusion(bf16[512,2048]{1,0:T(8,128)(2,1)S(1)} %bitcast.115, f32[512,256]{1,0:T(8,128)S(1)} %fusion.13, f32[512,256]{1,0:T(8,128)S(1)} %fusion.10), kind=kOutput, calls=%fused_computation.6 | convolution fusion | flops 538181632 | bytes 4194304 | tf_op jit(solution)/shard_map/dot_general | solution.py:447
  67.6 2.1 %add_convert_fusion = bf16[512,2048]{1,0:T(8,128)(2,1)} fusion(f32[512,2048]{1,0:T(8,128)S(1)} %fusion.8, bf16[512,256]{1,0:T(8,128)(2,1)S(1)} %get-tuple-element.61, bf16[1,2048,256]{2,1,0:T(8,128)(2,1)S(1)} %copy-done.3), kind=kOutput, calls=%fused_computation | convolution fusion | flops 538968064 | bytes 7602176 | tf_op jit(solution)/shard_map/dot_general | solution.py:453
  69.7 0.8 fusion.53.pick_ref
  71.1 35.4 %giveback.1 = (bf16[128,2048]{1,0:T(8,128)(2,1)}, bf16[128,512]{1,0:T(8,128)(2,1)}, bf16[8,128,256]{2,1,0:T(8,128)(2,1)}) custom-call(bf16[8,64,2048]{2,1,0:T(8,128)(2,1)} %bitcast.113, bf16[128,512]{1,0:T(8,128)(2,1)} %fusion.53.pick_ref, bf16[128,512]{1,0:T(8,128)(2,1)} %copy-done.2, bf16[128,256]{1,0:T(8,128)(2,1)} %fusion.29.gated_ref), custom_call_target="tpu_custom_call" | custom-call | tf_op jit(solution)/shard_map/giveback/pallas_call | solution.py:357
  106.5 2.2 %fusion.31 = (bf16[128,256]{1,0:T(8,128)(2,1)}, f32[128,256]{1,0:T(8,128)S(1)}) fusion(bf16[128,256]{1,0:T(8,128)(2,1)S(1)} %copy-done.10, bf16[128,256]{1,0:T(8,128)(2,1)S(1)} %copy-done.11, bf16[128,2048]{1,0:T(8,128)(2,1)} %get-tuple-element.18, bf16[256,2048]{1,0:T(8,128)(2,1)S(1)} %copy-done.16), kind=kOutput, calls=%fused_computation.59 | convolution fusion | flops 134676480 | bytes 1900544 | tf_op jit(solution)/shard_map/dot_general | solution.py:453
  109.3 0.9 convolution_convert_fusion.5.grad_ref
  110.8 0.9 constant_dynamic-slice_fusion
  112.4 21.2 %later.1 = (f32[4,64,128]{2,1,0:T(8,128)}, bf16[8,4,32,256]{3,2,1,0:T(8,128)(2,1)}) custom-call(bf16[4,64,128]{2,1,0:T(8,128)(2,1)} %convolution_convert_fusion.5.grad_ref, f32[4,128]{1,0:T(4,128)} %broadcast_in_dim.45.decay_ref, bf16[8,32,256]{2,1,0:T(8,128)(2,1)} %bitcast.124), custom_call_target="tpu_custom_call" | custom-call | tf_op jit(solution)/shard_map/later/pallas_call | solution.py:423
  133.6 2.1 %fusion.65 = f32[256,256]{1,0:T(8,128)} fusion(bf16[1024,256]{1,0:T(8,128)(2,1)} %bitcast.123, bf16[1024,256]{1,0:T(8,128)(2,1)S(1)} %bitcast.121), kind=kOutput, calls=%fused_computation.106 | convolution fusion | flops 134217728 | bytes 1310720 | tf_op jit(solution)/shard_map/dot_general | solution.py:447
  135.8 1.2 fusion.6
  137.7 0.7 copy.71
  139.4 0.9 convolution_add_fusion.1
  140.7 0.8 convolution_add_fusion
  (69 shorter events, 9.4 us)
Async XLA Ops:
  0.6 55.7 %copy-start = (bf16[1,2048,256]{2,1,0:T(8,128)(2,1)S(1)}, bf16[1,2048,256]{2,1,0:T(8,128)(2,1)}, u32[]{:S(2)}) copy-start(bf16[1,2048,256]{2,1,0:T(8,128)(2,1)} %param.19) | copy-start | bytes 3145732
  7.7 51.2 %copy-start.2 = (bf16[128,512]{1,0:T(8,128)(2,1)}, bf16[128,512]{1,0:T(8,128)(2,1)S(1)}, u32[]{:S(2)}) copy-start(bf16[128,512]{1,0:T(8,128)(2,1)S(1)} %get-tuple-element.60.cot_ref) | copy-start | bytes 393220
  56.4 2.5 %copy-start.3 = (bf16[1,2048,256]{2,1,0:T(8,128)(2,1)S(1)}, bf16[1,2048,256]{2,1,0:T(8,128)(2,1)}, u32[]{:S(2)}) copy-start(bf16[1,2048,256]{2,1,0:T(8,128)(2,1)} %param.20) | copy-start | bytes 3145732
  56.4 2.5 %copy-start.14 = (bf16[8,64,2048]{2,1,0:T(8,128)(2,1)S(1)}, bf16[8,64,2048]{2,1,0:T(8,128)(2,1)}, u32[]{:S(2)}) copy-start(bf16[8,64,2048]{2,1,0:T(8,128)(2,1)} %get-tuple-element.16) | copy-start | bytes 6291460
  58.9 1.6 %copy-start.1 = (bf16[8,64,2048]{2,1,0:T(8,128)(2,1)S(1)}, bf16[8,64,2048]{2,1,0:T(8,128)(2,1)}, u32[]{:S(2)}) copy-start(bf16[8,64,2048]{2,1,0:T(8,128)(2,1)} %get-tuple-element.17) | copy-start | bytes 6291460
  58.9 1.9 %copy-start.15 = (bf16[1,256,2048]{2,1,0:T(8,128)(2,1)S(1)}, bf16[1,256,2048]{2,1,0:T(8,128)(2,1)}, u32[]{:S(2)}) copy-start(bf16[1,256,2048]{2,1,0:T(8,128)(2,1)} %param.21) | copy-start | bytes 3145732
  67.6 2.9 %copy-start.10 = (bf16[128,256]{1,0:T(8,128)(2,1)S(1)}, bf16[128,256]{1,0:T(8,128)(2,1)}, u32[]{:S(2)}) copy-start(bf16[128,256]{1,0:T(8,128)(2,1)} %param.24) | copy-start | bytes 196612
  67.6 2.9 %copy-start.11 = (bf16[128,256]{1,0:T(8,128)(2,1)S(1)}, bf16[128,256]{1,0:T(8,128)(2,1)}, u32[]{:S(2)}) copy-start(bf16[128,256]{1,0:T(8,128)(2,1)} %param.23) | copy-start | bytes 196612
  69.7 36.8 %copy-start.16 = (bf16[256,2048]{1,0:T(8,128)(2,1)S(1)}, bf16[256,2048]{1,0:T(8,128)(2,1)}, u32[]{:S(2)}) copy-start(bf16[256,2048]{1,0:T(8,128)(2,1)} %param.22) | copy-start | bytes 3145732
  71.1 37.7 %copy-start.13 = (f32[4,128]{1,0:T(4,128)S(1)}, f32[4,128]{1,0:T(4,128)}, u32[]{:S(2)}) copy-start(f32[4,128]{1,0:T(4,128)} %param.28) | copy-start | bytes 6148
  71.1 38.1 %copy-start.6 = (bf16[128,128]{1,0:T(8,128)(2,1)S(1)}, bf16[128,128]{1,0:T(8,128)(2,1)}, u32[]{:S(2)}) copy-start(bf16[128,128]{1,0:T(8,128)(2,1)} %param.27) | copy-start | bytes 98308
  106.5 27.1 %copy-start.5 = (bf16[8,128,256]{2,1,0:T(8,128)(2,1)S(1)}, bf16[8,128,256]{2,1,0:T(8,128)(2,1)}, u32[]{:S(2)}) copy-start(bf16[8,128,256]{2,1,0:T(8,128)(2,1)} %get-tuple-element.20) | copy-start | bytes 1572868
  108.8 27.0 %copy-start.7 = (bf16[128,128]{1,0:T(8,128)(2,1)S(1)}, bf16[128,128]{1,0:T(8,128)(2,1)}, u32[]{:S(2)}) copy-start(bf16[128,128]{1,0:T(8,128)(2,1)} %param.26) | copy-start | bytes 98308
  108.8 29.7 %copy-start.12 = (bf16[128,256]{1,0:T(8,128)(2,1)S(1)}, bf16[128,256]{1,0:T(8,128)(2,1)}, u32[]{:S(2)}) copy-start(bf16[128,256]{1,0:T(8,128)(2,1)} %param.25) | copy-start | bytes 196612
  111.7 28.6 %copy-start.8 = (f32[1,4,64,128]{3,2,1,0:T(8,128)S(1)}, f32[1,4,64,128]{3,2,1,0:T(8,128)}, u32[]{:S(2)}) copy-start(f32[1,4,64,128]{3,2,1,0:T(8,128)} %param.29) | copy-start | bytes 393220
  133.6 5.0 %copy-start.4 = (f32[4,64,128]{2,1,0:T(8,128)S(1)}, f32[4,64,128]{2,1,0:T(8,128)}, u32[]{:S(2)}) copy-start(f32[4,64,128]{2,1,0:T(8,128)} %get-tuple-element.22) | copy-start | bytes 393220
  133.6 7.9 %copy-start.9 = (bf16[128,512]{1,0:T(8,128)(2,1)S(1)}, bf16[128,512]{1,0:T(8,128)(2,1)}, u32[]{:S(2)}) copy-start(bf16[128,512]{1,0:T(8,128)(2,1)} %get-tuple-element.86) | copy-start | bytes 393220

commit v2 on v1

--- a/solution.py
+++ b/solution.py
@@ -29,7 +29,7 @@
     return (i // 2 + 1) * (1 - 2 * (i % 2))
 
 
-def greet(n, m, me, t):
+def announce(n, m, me, t):
     barrier = pltpu.get_barrier_semaphore()
 
     @pl.loop(1, n)
@@ -41,7 +41,15 @@
         pl.semaphore_signal(barrier, inc=1, device_id=(me, (t + 2 * d) % m), device_id_type=MESH_ID)
 
     pl.semaphore_signal(barrier, inc=1, device_id=(me, sibling(t)), device_id_type=MESH_ID)
-    pl.semaphore_wait(barrier, n - 1 + m // 2)
+
+
+def await_all(n, m):
+    pl.semaphore_wait(pltpu.get_barrier_semaphore(), n - 1 + m // 2)
+
+
+def greet(n, m, me, t):
+    announce(n, m, me, t)
+    await_all(n, m)
 
 
 def sibling(t):
@@ -166,13 +174,42 @@
                 self.arrived(j, (sibling(self.t) + 2 * d) % m)
 
 
-def dispatch_kernel(n, m, tok_ref, cot_ref, tok_out, cot_out, *sems):
+def dispatch_kernel(
+    n, m, mixed_ref, cot_ref, routes_ref, gates_ref,
+    tok_out, cot_out, pick_out, tok_buf, cot_buf, *sems,
+):
     me, t = lax.axis_index("sp"), lax.axis_index("tp")
-    width = tok_ref.shape[2]
+    f32, bf16 = jnp.float32, jnp.bfloat16
+    cap, width = tok_buf.shape[1:]
     half = len(sems) // 2
-    tok = Spread(n, m, me, t, tok_ref, lambda j, q: tok_out.at[j, :, cols(q, width)], sems[:half])
-    cot = Spread(n, m, me, t, cot_ref, lambda j, q: cot_out.at[j, :, cols(q, width)], sems[half:])
-    greet(n, m, me, t)
+    announce(n, m, me, t)
+    routes, gates = routes_ref[...], gates_ref[...]
+    rows = routes.shape[0]
+    expert = lax.broadcasted_iota(jnp.int32, (rows, n), 1)
+    hot = [(routes[:, k : k + 1] == expert).astype(f32) for k in range(TOPK)]
+    later = lax.broadcasted_iota(jnp.int32, (rows, rows), 0)
+    sooner = lax.broadcasted_iota(jnp.int32, (rows, rows), 1)
+    counts = jnp.dot(
+        (later > sooner).astype(bf16), sum(hot[1:], hot[0]).astype(bf16), preferred_element_type=f32
+    )
+    slots = lax.broadcasted_iota(jnp.int32, (rows, n * cap), 1).astype(f32)
+    chosen = []
+    for k in range(TOPK):
+        slot = jnp.sum(hot[k] * counts, axis=1, keepdims=True)
+        target = routes[:, k : k + 1].astype(f32) * cap + slot
+        chosen.append((target == slots).astype(f32).astype(bf16))
+        counts = counts + hot[k]
+    pick = sum(chosen[1:], chosen[0])
+    tok = contract_rows(pick, mixed_ref[:, cols(t, width)])
+    tok_buf[...] = tok.astype(bf16).reshape(n, cap, width)
+    cotangent = cot_ref[:, cols(t, width)].astype(f32)
+    scaled = [(gates[:, k : k + 1] * cotangent).astype(bf16) for k in range(TOPK)]
+    cot = sum(contract_rows(chosen[k], scaled[k]) for k in range(TOPK))
+    cot_buf[...] = cot.astype(bf16).reshape(n, cap, width)
+    pick_out[...] = pick
+    tok = Spread(n, m, me, t, tok_buf, lambda j, q: tok_out.at[j, :, cols(q, width)], sems[:half])
+    cot = Spread(n, m, me, t, cot_buf, lambda j, q: cot_out.at[j, :, cols(q, width)], sems[half:])
+    await_all(n, m)
     tok.begin()
     tok.begin_own()
     cot.begin()
@@ -183,18 +220,19 @@
     cot.finish()
 
 
-def dispatch(n, m, tok_buffer, cot_buffer):
-    cap, width = tok_buffer.shape[1:]
-    out = jax.ShapeDtypeStruct((n, cap, width * m), tok_buffer.dtype)
+def dispatch(n, m, cap, mixed, cotangent, routes, gates):
+    rows, depth = mixed.shape
+    bf16 = jnp.bfloat16
+    out = jax.ShapeDtypeStruct((n, cap, depth), bf16)
     return pl.pallas_call(
         functools.partial(dispatch_kernel, n, m),
-        out_shape=(out, out),
-        in_specs=[VMEM] * 2,
-        out_specs=(VMEM, VMEM),
-        scratch_shapes=Spread.scratch(n, m) * 2,
+        out_shape=(out, out, jax.ShapeDtypeStruct((rows, n * cap), bf16)),
+        in_specs=[VMEM] * 4,
+        out_specs=(VMEM,) * 3,
+        scratch_shapes=[pltpu.VMEM((n, cap, depth // m), bf16)] * 2 + Spread.scratch(n, m) * 2,
         compiler_params=pltpu.CompilerParams(collective_id=0, has_side_effects=True),
         name="dispatch",
-    )(tok_buffer, cot_buffer)
+    )(mixed, cotangent, routes, gates)
 
 
 def giveback_kernel(
@@ -202,11 +240,11 @@
     whole_out, slice_out, gated_out,
     sib, away, near, leave, back,
     sib_send, sib_recv, away_send, near_recv, leave_send, back_recv,
-    gated_send, gated_recv, gated_own, share_send, share_recv, relay_send,
+    gated_send, gated_recv, gated_own, gated_relay, share_send, share_recv, relay_send,
 ):
     me, t = lax.axis_index("sp"), lax.axis_index("tp")
     half = m // 2
-    width = cot_ref.shape[1]
+    width = cot_ref.shape[1] // m
     cap = part_ref.shape[1]
     other = sibling(t)
     f32 = jnp.float32
@@ -236,6 +274,14 @@
     def to_home(j):
         return remote(leave.at[j], back.at[me], leave_send.at[j], back_recv.at[me], (j, t))
 
+    def gated_on(j):
+        spot = gated_out.at[j]
+        return remote(spot, spot, gated_relay.at[j], gated_recv.at[j], (sibling(me), t))
+
+    def gated_in(j):
+        spot = gated_out.at[j]
+        remote(spot, spot, gated_send.at[j], gated_recv.at[j], (me, t)).wait_recv()
+
     order = lambda i: (me + signed_step(n - 2 - i) + n) % n
 
     for d in list(range(1, half)) + [0]:
@@ -243,9 +289,11 @@
     keep = pltpu.make_async_copy(gated_ref, gated_out.at[me], gated_own.at[0])
     keep.start()
 
-    @pl.loop(0, n - 1)
-    def _(i):
-        to_gated(order(i)).start()
+    to_gated(sibling(me)).start()
+
+    @pl.loop(1, n // 2)
+    def _(k):
+        to_gated((me + 2 * k) % n).start()
 
     for d in list(range(1, half)) + [0]:
         to_sibling(d).wait_recv()
@@ -291,6 +339,12 @@
     back[me] = total(me)
     to_home(order(n - 2)).start()
 
+    @pl.loop(1, n // 2)
+    def _(k):
+        j = (me - 2 * k + n) % n
+        gated_in(j)
+        gated_on(j).start()
+
     @pl.loop(0, n - 1)
     def _(i):
         j = order(i)
@@ -298,7 +352,7 @@
         remote(spot, spot, leave_send.at[j], back_recv.at[j], (me, t)).wait_recv()
 
     added = jnp.dot(pick_ref[...], back[...].reshape(n * cap, width), preferred_element_type=f32)
-    result = (cot_ref[...].astype(f32) + added).astype(jnp.bfloat16)
+    result = (cot_ref[:, cols(t, width)].astype(f32) + added).astype(jnp.bfloat16)
     slice_out[...] = result
     whole_out[:, cols(t, width)] = result
 
@@ -336,10 +390,16 @@
     @pl.loop(0, n - 1)
     def _(i):
         j = order(i)
-        to_gated(j).wait_send()
         to_home(j).wait_send()
-        spot = gated_out.at[j]
-        remote(spot, spot, gated_send.at[j], gated_recv.at[j], (me, t)).wait_recv()
+
+    to_gated(sibling(me)).wait_send()
+    gated_in(sibling(me))
+
+    @pl.loop(1, n // 2)
+    def _(k):
+        to_gated((me + 2 * k) % n).wait_send()
+        gated_on((me - 2 * k + n) % n).wait_send()
+        gated_in((sibling(me) + 2 * k) % n)
 
     @pl.loop(0, n)
     def _(j):
@@ -349,9 +409,9 @@
     keep.wait()
 
 
-def giveback(n, m, part, pick, cot_slice, gated):
+def giveback(n, m, part, pick, cotangent, gated):
     cap = part.shape[1]
-    rows, width = cot_slice.shape
+    rows, width = cotangent.shape[0], cotangent.shape[1] // m
     half = m // 2
     bf16, dma = jnp.bfloat16, pltpu.SemaphoreType.DMA
     return pl.pallas_call(
@@ -370,16 +430,16 @@
             pltpu.VMEM((n, cap, width), bf16),
             pltpu.VMEM((n, cap, width), bf16),
             dma((half,)), dma((half,)), dma((half, n)), dma((half, n)), dma((n,)), dma((n,)),
-            dma((n,)), dma((n,)), dma((1,)), dma((half,)), dma((m,)), dma((half,)),
+            dma((n,)), dma((n,)), dma((1,)), dma((n,)), dma((half,)), dma((m,)), dma((half,)),
         ],
         compiler_params=pltpu.CompilerParams(collective_id=1, has_side_effects=True),
         name="giveback",
-    )(part, pick, cot_slice, gated)
+    )(part, pick, cotangent, gated)
 
 
 def later_kernel(
     n, m, grad_ref, decay_ref, rows_ref, state_out, rows_out,
-    held, rates, grad_send, grad_recv, rate_send, rate_recv, *sems,
+    held, rates, near, far, grad_send, grad_recv, rate_send, rate_recv, pair_send, pair_recv, *sems,
 ):
     me, t = lax.axis_index("sp"), lax.axis_index("tp")
     rows = Spread(n, m, me, t, rows_ref, lambda j, q: rows_out.at[j, q], sems)
@@ -391,29 +451,69 @@
     def rate_to(p):
         return remote(decay_ref, rates.at[me], rate_send.at[p], rate_recv.at[me], (p, t))
 
-    rows.begin()
-    rows.begin_own()
+    def grad_in(j):
+        spot = held.at[j]
+        remote(spot, spot, grad_send.at[j], grad_recv.at[j], (me, t)).wait_recv()
+
+    odd = me % 2
 
     @pl.loop(0, me)
     def _(p):
         rate_to(p).start()
-        grad_to(p).start()
-
+
+    @pl.when(odd == 1)
+    def _():
+        grad_to(me - 1).start()
+
+    @pl.loop(1, me // 2 + 1)
+    def _(k):
+        grad_to(me - 2 * k).start()
+
+    rows.begin()
+    rows.begin_own()
     rows.hand_on()
     state_out[...] = jnp.zeros_like(state_out)
 
-    @pl.loop(0, n - 1 - me)
+    @pl.loop(me + 1, n)
+    def _(j):
+        rate = rates.at[j]
+        remote(rate, rate, rate_send.at[j], rate_recv.at[j], (me, t)).wait_recv()
+
+    @pl.loop(0, n // 2 - 1 - me // 2)
     def _(i):
-        j = n - 1 - i
-        spot, rate = held.at[j], rates.at[j]
-        remote(rate, rate, rate_send.at[j], rate_recv.at[j], (me, t)).wait_recv()
-        remote(spot, spot, grad_send.at[j], grad_recv.at[j], (me, t)).wait_recv()
-        state_out[...] = rates[j][:, None, :] * state_out[...] + held[j].astype(jnp.float32)
+        even = n - 2 - 2 * i
+        j = even + odd
+        grad_in(j)
+        first, second = rates[even], rates[even + 1]
+        lead = jnp.where(odd == 1, first, jnp.ones_like(first))
+        state_out[...] = (first * second)[:, None, :] * state_out[...] + lead[
+            :, None, :
+        ] * held[j].astype(jnp.float32)
+
+    near[...] = state_out[...].astype(near.dtype)
+    swap = remote(near, far, pair_send.at[0], pair_recv.at[0], (sibling(me), t))
+    swap.start()
+    swap.wait()
+    state_out[...] = state_out[...] + far[...].astype(jnp.float32)
+
+    @pl.when(odd == 0)
+    def _():
+        grad_in(me + 1)
+        state_out[...] = rates[me + 1][:, None, :] * state_out[...] + held[me + 1].astype(
+            jnp.float32
+        )
 
     @pl.loop(0, me)
     def _(p):
         rate_to(p).wait_send()
-        grad_to(p).wait_send()
+
+    @pl.when(odd == 1)
+    def _():
+        grad_to(me - 1).wait_send()
+
+    @pl.loop(1, me // 2 + 1)
+    def _(k):
+        grad_to(me - 2 * k).wait_send()
 
     rows.finish()
 
@@ -431,7 +531,9 @@
         scratch_shapes=[
             pltpu.VMEM((n,) + grad.shape, grad.dtype),
             pltpu.VMEM((n,) + decay.shape, decay.dtype),
-            dma((n,)), dma((n,)), dma((n,)), dma((n,)),
+            pltpu.VMEM(grad.shape, grad.dtype),
+            pltpu.VMEM(grad.shape, grad.dtype),
+            dma((n,)), dma((n,)), dma((n,)), dma((n,)), dma((1,)), dma((1,)),
         ] + Spread.scratch(n, m),
         compiler_params=pltpu.CompilerParams(collective_id=2, has_side_effects=True),
         name="later",
@@ -501,35 +603,11 @@
     sp_count = lax.axis_size("sp")
     tp_count = lax.axis_size("tp")
     capacity = 4 * TOK_DEV // sp_count
-    assigned = TOK_DEV * TOPK
-    picks = routes.reshape(assigned)
-    onehot = (picks[:, None] == jnp.arange(sp_count, dtype=jnp.int32)[None, :]).astype(jnp.int32)
-    earlier_same = jnp.cumsum(onehot, axis=0) - onehot
-    slot_of = jnp.sum(earlier_same * onehot, axis=1)
-    target = (picks * capacity + slot_of).reshape(TOK_DEV, TOPK)
-    slots = jnp.arange(sp_count * capacity, dtype=jnp.int32)[None, :]
-    chosen = [(target[:, k : k + 1] == slots).astype(jnp.bfloat16) for k in range(TOPK)]
-    pick = sum(chosen[1:], chosen[0])
     weight_g = w_gate[0]
     weight_u = w_up[0]
     weight_d = w_down[0]
-    column_count = D // tp_count
-    offset = lax.axis_index("tp") * column_count
-    tok_slice = lax.dynamic_slice_in_dim(mixed, offset, column_count, 1)
-    cot_slice = lax.dynamic_slice_in_dim(cotangent, offset, column_count, 1)
-    scaled = [
-        (gates[:, k : k + 1] * cot_slice.astype(jnp.float32)).astype(jnp.bfloat16)
-        for k in range(TOPK)
-    ]
-    tok_buffer = contract_rows(pick, tok_slice).astype(jnp.bfloat16)
-    cot_buffer = contract_rows(
-        jnp.concatenate(chosen, axis=0), jnp.concatenate(scaled, axis=0)
-    ).astype(jnp.bfloat16)
-    expert_tok_rows, expert_cot_rows = dispatch(
-        sp_count,
-        tp_count,
-        tok_buffer.reshape(sp_count, capacity, column_count),
-        cot_buffer.reshape(sp_count, capacity, column_count),
+    expert_tok_rows, expert_cot_rows, pick = dispatch(
+        sp_count, tp_count, capacity, mixed, cotangent, routes, gates
     )
     expert_tok_rows = expert_tok_rows.reshape(-1, D)
     expert_cot_rows = expert_cot_rows.reshape(-1, D)
@@ -553,7 +631,7 @@
         tp_count,
         partial_value.astype(jnp.bfloat16).reshape(sp_count, capacity, D),
         pick,
-        cot_slice,
+        cotangent,
         gated,
     )
     back_proj = contract_cols(whole, out_weight)

time: 142 us -> 140 us (0.986)
  Pallas kernels: 104 us -> 108 us
  other arithmetic: 4.29 us -> 0.92 us
  matrix products: 25.1 us -> 21.9 us
    pallas_call x1, Pallas kernels: 21.2 us -> 27.2 us  [later(): pl.pallas_call(functools.partial(later_kernel, n, m), out_shape=(jax.Shap...]
    dot_general x6 -> x4, matrix products: 10.6 us -> 7.37 us  [contract_rows(): lax.dot_general(first_op, second_op, (((0,), (0,)), ((), ())), preferred_...]
    pallas_call x1, Pallas kernels: 35.4 us -> 32.9 us  [giveback(): pl.pallas_call(functools.partial(giveback_kernel, n, m), out_shape=(jax.S...]
    unnamed x38 -> x37, local copies, waits for them, and re-layouts: 3.62 us -> 5.66 us
    add x2 -> x0, other arithmetic: 1.48 us -> none  [the longest x1 0.77 us: body(): pick = sum(chosen[1:], chosen[0])]
where the time goes in v2:
time: 140 us
  Pallas kernels  108 us (77%)
  matrix products  21.9 us (16%)
  local copies, waits for them, and re-layouts  8.29 us (6%)
    pallas_call x1, Pallas kernels, dispatch(): pl.pallas_call(functools.partial(dispatch_kernel, n, m), out_shape=(out,...  47.7 us
    pallas_call x1, Pallas kernels, giveback(): pl.pallas_call(functools.partial(giveback_kernel, n, m), out_shape=(jax.S...  32.9 us
    pallas_call x1, Pallas kernels, later(): pl.pallas_call(functools.partial(later_kernel, n, m), out_shape=(jax.Shap...  27.2 us
    dot_general x4, matrix products, contract_rows(): lax.dot_general(first_op, second_op, (((0,), (0,)), ((), ())), preferred_...  7.37 us
    dot_general x4, matrix products, contract_cols(): lax.dot_general(first_op, second_op, (((1,), (1,)), ((), ())), preferred_...  5.86 us
    unnamed x37, local copies, waits for them, and re-layouts  5.66 us

profile of v2, /device:TPU:0, one launch (start us, length us, event | category | flops | bytes accessed | tf_op | source)
XLA Modules:
  0.0 139.8 jit_solution(13479025061221966363)
XLA Ops:
  0.7 1.5 %copy.36.routes_ref = s32[128,2]{1,0:T(8,128)} copy(s32[128,2]{0,1:T(2,128)} %param.17) | data formatting | bytes 2048 | tf_op args[2]
  2.2 1.4 %copy.37.gates_ref = f32[128,2]{1,0:T(8,128)} copy(f32[128,2]{0,1:T(2,128)} %param.18) | data formatting | bytes 2048 | tf_op args[3]
  3.6 47.7 %dispatch.1 = (bf16[8,64,2048]{2,1,0:T(8,128)(2,1)}, bf16[8,64,2048]{2,1,0:T(8,128)(2,1)}, bf16[128,512]{1,0:T(8,128)(2,1)}) custom-call(bf16[128,2048]{1,0:T(8,128)(2,1)} %mixed_ref.1, bf16[128,2048]{1,0:T(8,128)(2,1)} %cot_ref.3, s32[128,2]{1,0:T(8,128)} %copy.36.routes_ref, f32[128,2]{1,0:T(8,128)} %copy.37.gates_ref), custom_call_target="tpu_custom_call" | custom-call | tf_op jit(solution)/shard_map/dispatch/pallas_call | solution.py:227
  51.3 2.5 %fusion.10 = f32[512,256]{1,0:T(8,128)S(1)} fusion(bf16[512,2048]{1,0:T(8,128)(2,1)} %bitcast.110, bf16[1,2048,256]{2,1,0:T(8,128)(2,1)S(1)} %copy-done), kind=kOutput, calls=%fused_computation.22 | convolution fusion | flops 536870912 | bytes 3670016 | tf_op jit(solution)/shard_map/dot_general | solution.py:614
  53.8 0.7 fusion.13
  54.5 0.9 copy-done.1
  55.7 0.8 multiply_convert_fusion.1
  56.5 1.7 %fusion = bf16[1,2048,256]{2,1,0:T(8,128)(2,1)} fusion(bf16[512,2048]{1,0:T(8,128)(2,1)S(1)} %bitcast.112, bf16[512,256]{1,0:T(8,128)(2,1)S(1)} %get-tuple-element.44), kind=kOutput, calls=%fused_computation.4 | convolution fusion | flops 537395200 | bytes 3407872 | tf_op jit(solution)/shard_map/dot_general | solution.py:549
  58.2 1.8 %fusion.1 = bf16[1,2048,256]{2,1,0:T(8,128)(2,1)} fusion(bf16[512,2048]{1,0:T(8,128)(2,1)S(1)} %bitcast.113, bf16[512,256]{1,0:T(8,128)(2,1)S(1)} %get-tuple-element.43), kind=kOutput, calls=%fused_computation.5 | convolution fusion | flops 537395200 | bytes 3407872 | tf_op jit(solution)/shard_map/dot_general | solution.py:549
  60.0 1.8 %fusion.2 = bf16[1,256,2048]{2,1,0:T(8,128)(2,1)} fusion(bf16[512,2048]{1,0:T(8,128)(2,1)S(1)} %bitcast.97, f32[512,256]{1,0:T(8,128)S(1)} %fusion.13, f32[512,256]{1,0:T(8,128)S(1)} %fusion.10), kind=kOutput, calls=%fused_computation.6 | convolution fusion | flops 538181632 | bytes 4194304 | tf_op jit(solution)/shard_map/dot_general | solution.py:549
  61.7 0.7 fusion.8
  62.5 2.1 %add_convert_fusion = bf16[512,2048]{1,0:T(8,128)(2,1)} fusion(f32[512,2048]{1,0:T(8,128)S(1)} %fusion.8, bf16[512,256]{1,0:T(8,128)(2,1)S(1)} %get-tuple-element.43, bf16[1,2048,256]{2,1,0:T(8,128)(2,1)S(1)} %copy-done.2), kind=kOutput, calls=%fused_computation | convolution fusion | flops 538968064 | bytes 7602176 | tf_op jit(solution)/shard_map/dot_general | solution.py:555
  64.6 0.7 fusion.19.gated_ref
  65.3 32.9 %giveback.1 = (bf16[128,2048]{1,0:T(8,128)(2,1)}, bf16[128,512]{1,0:T(8,128)(2,1)}, bf16[8,128,256]{2,1,0:T(8,128)(2,1)}) custom-call(bf16[8,64,2048]{2,1,0:T(8,128)(2,1)} %bitcast.95, bf16[128,512]{1,0:T(8,128)(2,1)} %get-tuple-element.19.pick_ref, bf16[128,2048]{1,0:T(8,128)(2,1)} %cot_ref.3, bf16[128,256]{1,0:T(8,128)(2,1)} %fusion.19.gated_ref), custom_call_target="tpu_custom_call" | custom-call | tf_op jit(solution)/shard_map/giveback/pallas_call | solution.py:417
  98.2 2.2 %fusion.21 = (bf16[128,256]{1,0:T(8,128)(2,1)}, f32[128,256]{1,0:T(8,128)S(1)}) fusion(bf16[128,256]{1,0:T(8,128)(2,1)S(1)} %copy-done.9, bf16[128,256]{1,0:T(8,128)(2,1)S(1)} %copy-done.10, bf16[128,2048]{1,0:T(8,128)(2,1)} %get-tuple-element.20, bf16[256,2048]{1,0:T(8,128)(2,1)S(1)} %copy-done.15), kind=kOutput, calls=%fused_computation.43 | convolution fusion | flops 134676480 | bytes 1900544 | tf_op jit(solution)/shard_map/dot_general | solution.py:555
  100.9 0.9 convolution_convert_fusion.3.grad_ref
  102.4 0.9 constant_dynamic-slice_fusion
  103.4 0.7 copy.49
  104.0 27.2 %later.1 = (f32[4,64,128]{2,1,0:T(8,128)}, bf16[8,4,32,256]{3,2,1,0:T(8,128)(2,1)}) custom-call(bf16[4,64,128]{2,1,0:T(8,128)(2,1)} %convolution_convert_fusion.3.grad_ref, f32[4,128]{1,0:T(4,128)} %broadcast_in_dim.43.decay_ref, bf16[8,32,256]{2,1,0:T(8,128)(2,1)} %bitcast.104), custom_call_target="tpu_custom_call" | custom-call | tf_op jit(solution)/shard_map/later/pallas_call | solution.py:523
  131.3 2.1 %fusion.47 = f32[256,256]{1,0:T(8,128)} fusion(bf16[1024,256]{1,0:T(8,128)(2,1)} %bitcast.103, bf16[1024,256]{1,0:T(8,128)(2,1)S(1)} %bitcast.102), kind=kOutput, calls=%fused_computation.73 | convolution fusion | flops 134217728 | bytes 1310720 | tf_op jit(solution)/shard_map/dot_general | solution.py:549
  133.5 1.2 fusion.6
  135.4 0.7 copy.46
  137.1 0.9 convolution_add_fusion.1
  138.4 0.8 convolution_add_fusion
  (49 shorter events, 4.3 us)
Async XLA Ops:
  0.6 50.6 %copy-start = (bf16[1,2048,256]{2,1,0:T(8,128)(2,1)S(1)}, bf16[1,2048,256]{2,1,0:T(8,128)(2,1)}, u32[]{:S(2)}) copy-start(bf16[1,2048,256]{2,1,0:T(8,128)(2,1)} %param.19) | copy-start | bytes 3145732
  51.2 2.5 %copy-start.2 = (bf16[1,2048,256]{2,1,0:T(8,128)(2,1)S(1)}, bf16[1,2048,256]{2,1,0:T(8,128)(2,1)}, u32[]{:S(2)}) copy-start(bf16[1,2048,256]{2,1,0:T(8,128)(2,1)} %param.20) | copy-start | bytes 3145732
  51.3 2.5 %copy-start.13 = (bf16[8,64,2048]{2,1,0:T(8,128)(2,1)S(1)}, bf16[8,64,2048]{2,1,0:T(8,128)(2,1)}, u32[]{:S(2)}) copy-start(bf16[8,64,2048]{2,1,0:T(8,128)(2,1)} %get-tuple-element.17) | copy-start | bytes 6291460
  53.8 1.6 %copy-start.1 = (bf16[8,64,2048]{2,1,0:T(8,128)(2,1)S(1)}, bf16[8,64,2048]{2,1,0:T(8,128)(2,1)}, u32[]{:S(2)}) copy-start(bf16[8,64,2048]{2,1,0:T(8,128)(2,1)} %get-tuple-element.18) | copy-start | bytes 6291460
  53.8 1.9 %copy-start.14 = (bf16[1,256,2048]{2,1,0:T(8,128)(2,1)S(1)}, bf16[1,256,2048]{2,1,0:T(8,128)(2,1)}, u32[]{:S(2)}) copy-start(bf16[1,256,2048]{2,1,0:T(8,128)(2,1)} %param.21) | copy-start | bytes 3145732
  62.5 2.1 %copy-start.9 = (bf16[128,256]{1,0:T(8,128)(2,1)S(1)}, bf16[128,256]{1,0:T(8,128)(2,1)}, u32[]{:S(2)}) copy-start(bf16[128,256]{1,0:T(8,128)(2,1)} %param.24) | copy-start | bytes 196612
  62.5 2.1 %copy-start.10 = (bf16[128,256]{1,0:T(8,128)(2,1)S(1)}, bf16[128,256]{1,0:T(8,128)(2,1)}, u32[]{:S(2)}) copy-start(bf16[128,256]{1,0:T(8,128)(2,1)} %param.23) | copy-start | bytes 196612
  64.6 33.6 %copy-start.15 = (bf16[256,2048]{1,0:T(8,128)(2,1)S(1)}, bf16[256,2048]{1,0:T(8,128)(2,1)}, u32[]{:S(2)}) copy-start(bf16[256,2048]{1,0:T(8,128)(2,1)} %param.22) | copy-start | bytes 3145732
  65.3 35.3 %copy-start.12 = (f32[4,128]{1,0:T(4,128)S(1)}, f32[4,128]{1,0:T(4,128)}, u32[]{:S(2)}) copy-start(f32[4,128]{1,0:T(4,128)} %param.28) | copy-start | bytes 6148
  98.2 2.8 %copy-start.5 = (bf16[128,128]{1,0:T(8,128)(2,1)S(1)}, bf16[128,128]{1,0:T(8,128)(2,1)}, u32[]{:S(2)}) copy-start(bf16[128,128]{1,0:T(8,128)(2,1)} %param.27) | copy-start | bytes 98308
  98.2 33.1 %copy-start.4 = (bf16[8,128,256]{2,1,0:T(8,128)(2,1)S(1)}, bf16[8,128,256]{2,1,0:T(8,128)(2,1)}, u32[]{:S(2)}) copy-start(bf16[8,128,256]{2,1,0:T(8,128)(2,1)} %get-tuple-element.22) | copy-start | bytes 1572868
  100.4 33.1 %copy-start.6 = (bf16[128,128]{1,0:T(8,128)(2,1)S(1)}, bf16[128,128]{1,0:T(8,128)(2,1)}, u32[]{:S(2)}) copy-start(bf16[128,128]{1,0:T(8,128)(2,1)} %param.26) | copy-start | bytes 98308
  100.4 35.7 %copy-start.11 = (bf16[128,256]{1,0:T(8,128)(2,1)S(1)}, bf16[128,256]{1,0:T(8,128)(2,1)}, u32[]{:S(2)}) copy-start(bf16[128,256]{1,0:T(8,128)(2,1)} %param.25) | copy-start | bytes 196612
  103.4 34.6 %copy-start.7 = (f32[1,4,64,128]{3,2,1,0:T(8,128)S(1)}, f32[1,4,64,128]{3,2,1,0:T(8,128)}, u32[]{:S(2)}) copy-start(f32[1,4,64,128]{3,2,1,0:T(8,128)} %param.29) | copy-start | bytes 393220
  131.3 5.0 %copy-start.3 = (f32[4,64,128]{2,1,0:T(8,128)S(1)}, f32[4,64,128]{2,1,0:T(8,128)}, u32[]{:S(2)}) copy-start(f32[4,64,128]{2,1,0:T(8,128)} %get-tuple-element.24) | copy-start | bytes 393220
  131.3 7.9 %copy-start.8 = (bf16[128,512]{1,0:T(8,128)(2,1)S(1)}, bf16[128,512]{1,0:T(8,128)(2,1)}, u32[]{:S(2)}) copy-start(bf16[128,512]{1,0:T(8,128)(2,1)} %get-tuple-element.62) | copy-start | bytes 393220
